TPU v7x, 256 devices: a whole 4x4x8 slice. The times are simulated.
256 devices in a mesh: sp: 64 (over z, x, core), tp: 4 (over y).
Axes of the slice: x: 4, y: 4, z: 8, core: 2. Of those that a mesh axis runs over, the one named last changes fastest.
Arguments:
- conv_in: bfloat16 [49152, 1024], P('sp', 'tp'), may hold values from -6 to 6
- conv_pre: bfloat16 [49152, 1024], P('sp', 'tp'), may hold values from -6 to 6
- conv_post: bfloat16 [49152, 1024], P('sp', 'tp'), may hold values from -6 to 6
- taps: float32 [3, 1024], P(None, 'tp'), may hold values from -3 to 3
- out_proj: bfloat16 [1024, 2048], P('tp'), may hold values from -0.1875 to 0.1875
- stream: bfloat16 [49152, 2048], P(('sp', 'tp')), may hold values from -6 to 6
- norm_gain: float32 [2048], replicated, may hold values from 0.1 to 1.9
- routes: int32 [49152, 2], P(('sp', 'tp')), may hold values from 0 to 63, all different within a row; in each aligned block of 192 rows (0 to 191, 192 to 383, ...) at most 8 rows name the same one
- route_weight: float32 [49152, 2], P(('sp', 'tp')), may hold values from 0.1 to 1
- gate_w: bfloat16 [64, 2048, 2048], P('sp', None, 'tp'), may hold values from -0.52734375 to 0.52734375
- up_w: bfloat16 [64, 2048, 2048], P('sp', None, 'tp'), may hold values from -0.52734375 to 0.52734375
- down_w: bfloat16 [64, 2048, 2048], P('sp', 'tp'), may hold values from -0.013244629 to 0.013244629
Outputs:
- output: bfloat16 [49152, 2048], P(('sp', 'tp'))
Inputs may be any that keep to these rules, and one draw needn't show every extreme that they name: `routes`: each row names 2 different experts. In each aligned block of 192 rows no expert is named more than 8 times, a bound that some block reaches.
All inputs are finite; a program needn't handle non-finite values.
Results may differ from a plain program's by a relative error of at most 0.015.
Values may be sent and summed in bfloat16 or wider, within the bound.
No kernel may reach another device: no remote copies, remote signals or barrier semaphores. Data moves between devices by JAX's collectives and lax.ppermute only.
A program may use at most 128 MiB of HBM per device.

v0:
```python
import jax
import jax.numpy as jnp
from jax import lax
from jax.experimental import pallas as pl
from jax.experimental.pallas import tpu as pltpu
from jax.sharding import PartitionSpec as P


EPSILON = 1e-05
LIMIT = 7.0
ALPHA = 1.702
CHUNKS = (4, 4)


def shift(x, by):
    count = lax.axis_size("tp")
    return lax.ppermute(x, "tp", [(i, (i + by) % count) for i in range(count)])


def core_swap(x):
    return lax.ppermute(x, "sp", [(i, i ^ 1) for i in range(lax.axis_size("sp"))])


def both(x, pairs):
    sp, tp = lax.axis_size("sp"), lax.axis_size("tp")
    every = []
    for chip in range(sp // 2):
        for (y0, c0), (y1, c1) in pairs:
            every.append(((2 * chip + c0) * tp + y0, (2 * chip + c1) * tp + y1))
    return lax.ppermute(x, ("sp", "tp"), every)


def roles(tp):
    host = [(y, y % 2) for y in range(tp)]
    guest = [(y, 1 - y % 2) for y in range(tp)]
    return host, guest


def weight_routes(tp):
    host, guest = roles(tp)
    over = [(host[y], guest[y]) for y in range(tp)]
    to_left = over + [(guest[y], host[(y - 1) % tp]) for y in range(tp)]
    to_right = over + [(guest[y], host[(y + 1) % tp]) for y in range(tp)]
    return to_left, to_right


def row_routes(tp):
    host, guest = roles(tp)
    first = [(guest[y], host[(y - 1) % tp]) for y in range(tp)]
    first += [(host[y], guest[(y + 2) % tp]) for y in range(tp)]
    second = [(guest[y], host[(y + 1) % tp]) for y in range(tp)]
    second += [(host[y], guest[y]) for y in range(tp)]
    return first, second


def flipped(pairs):
    return [(b, a) for a, b in pairs]


def dot(a, b):
    return jnp.dot(a, b, preferred_element_type=jnp.float32)


def clamped_unit(gate_pre, up_pre):
    gated = jnp.minimum(gate_pre, LIMIT)
    upward = jnp.clip(up_pre, -LIMIT, LIMIT)
    return (upward + 1.0) * gated * jax.nn.sigmoid(ALPHA * gated)


BLOCK = 256


def blocks(length, size):
    def over(body):
        @pl.loop(0, length // size)
        def _(step):
            body(pl.ds(pl.multiple_of(step * size, size), size))

    return over


def ffn_kernel(rows, gu_low, gu_high, down_low, down_high, *rest):
    *rest, pre, active = rest
    met, outs = (rest[0], rest[1:]) if len(rest) == 3 else (None, rest)
    count, width = rows.shape
    unit = down_low.shape[0]
    each = count // len(outs)

    for k, gu in enumerate((gu_low, gu_high)):

        @blocks(count, 64)
        def _(at):
            pre[at, :] = jnp.zeros((at.size, 2 * unit), jnp.float32)

        @blocks(width, BLOCK)
        def _(at):
            pre[...] += dot(rows[:, at], gu[at, :])

        @blocks(count, 32)
        def _(at):
            active[k, at, :] = clamped_unit(pre[at, :unit], pre[at, unit:]).astype(jnp.bfloat16)

    @blocks(width, BLOCK)
    def _(at):
        total = dot(active[0], down_low[:, at]) + dot(active[1], down_high[:, at])
        if met is not None:
            total = total + met[:, at].astype(jnp.float32)
        total = total.astype(jnp.bfloat16)
        for k, out in enumerate(outs):
            out[:, at] = total[k * each : (k + 1) * each]


def ffn(rows, low, high, met=None):
    number, width = rows.shape
    unit = low[1].shape[0]
    count = 1 if met is None else 2
    shape = jax.ShapeDtypeStruct((number // count, width), jnp.bfloat16)
    operands = (rows, low[0], high[0], low[1], high[1]) + (() if met is None else (met,))
    return pl.pallas_call(
        ffn_kernel,
        out_shape=(shape,) * count,
        in_specs=[pl.BlockSpec(memory_space=pltpu.VMEM)] * len(operands),
        out_specs=(pl.BlockSpec(memory_space=pltpu.VMEM),) * count,
        scratch_shapes=[
            pltpu.VMEM((number, 2 * unit), jnp.float32),
            pltpu.VMEM((2, number, unit), jnp.bfloat16),
        ],
        compiler_params=pltpu.CompilerParams(vmem_limit_bytes=32 * 2**20),
        cost_estimate=pl.CostEstimate(
            flops=2 * number * width * 6 * unit,
            bytes_accessed=4 * number * width + 12 * unit * width,
            transcendentals=2 * number * unit,
        ),
    )(*operands)


def sum_kernel(a, b, out):
    @blocks(a.shape[0], 32)
    def _(at):
        total = a[at, :].astype(jnp.float32) + b[at, :].astype(jnp.float32)
        out[at, :] = total.astype(out.dtype)


def sum_of(a, b):
    return pl.pallas_call(
        sum_kernel,
        out_shape=jax.ShapeDtypeStruct(a.shape, a.dtype),
        in_specs=[pl.BlockSpec(memory_space=pltpu.VMEM)] * 2,
        out_specs=pl.BlockSpec(memory_space=pltpu.VMEM),
        compiler_params=pltpu.CompilerParams(vmem_limit_bytes=8 * 2**20),
        cost_estimate=pl.CostEstimate(
            flops=a.size, bytes_accessed=3 * 2 * a.size, transcendentals=0
        ),
    )(a, b)


def combine_kernel(resid, first, second, places, weight, out, picks):
    shape = picks.shape[1:]
    ids = lax.broadcasted_iota(jnp.int32, shape, 1)
    for at in range(4):
        mine = places[:, at : at + 1] == ids
        picks[at] = jnp.where(mine, 1.0, 0.0).astype(jnp.bfloat16)

    @blocks(resid.shape[1], BLOCK)
    def _(at):
        total = resid[:, at].astype(jnp.float32)
        for k in range(2):
            picked = dot(picks[k], first[:, at]) + dot(picks[2 + k], second[:, at])
            total = total + weight[:, k : k + 1] * picked
        out[:, at] = total.astype(out.dtype)


def combine(resid, first, second, places, weight):
    rows, width = resid.shape
    number = first.shape[0]
    return pl.pallas_call(
        combine_kernel,
        out_shape=jax.ShapeDtypeStruct(resid.shape, resid.dtype),
        in_specs=[pl.BlockSpec(memory_space=pltpu.VMEM)] * 5,
        out_specs=pl.BlockSpec(memory_space=pltpu.VMEM),
        scratch_shapes=[pltpu.VMEM((4, rows, number), jnp.bfloat16)],
        compiler_params=pltpu.CompilerParams(vmem_limit_bytes=16 * 2**20),
        cost_estimate=pl.CostEstimate(
            flops=8 * rows * number * width,
            bytes_accessed=4 * (rows + number) * width,
            transcendentals=0,
        ),
    )(resid, first, second, places, weight)


def fill_kernel(resid, gain, places, *rest):
    *outs, picks = rest
    rows, width = resid.shape
    ids = lax.broadcasted_iota(jnp.int32, picks.shape[1:], 0)
    for c in range(len(outs)):
        mine = (places[2 * c : 2 * c + 1, :] == ids) | (places[2 * c + 1 : 2 * c + 2, :] == ids)
        picks[c] = jnp.where(mine, 1.0, 0.0).astype(jnp.bfloat16)

    def add(step, total):
        at = pl.ds(pl.multiple_of(step * BLOCK, BLOCK), BLOCK)
        part = resid[:, at].astype(jnp.float32)
        return total + jnp.sum(part * part, axis=1, keepdims=True)

    square = lax.fori_loop(0, width // BLOCK, add, jnp.zeros((rows, 1), jnp.float32))
    scale = lax.rsqrt(square / width + EPSILON)

    @blocks(width, BLOCK)
    def _(at):
        normed = resid[:, at].astype(jnp.float32) * scale * gain[:, at]
        normed = normed.astype(jnp.bfloat16)
        for c, out in enumerate(outs):
            out[:, at] = dot(picks[c], normed).astype(out.dtype)


def fill(resid, gain, places, sizes):
    rows, width = resid.shape
    return pl.pallas_call(
        fill_kernel,
        out_shape=tuple(jax.ShapeDtypeStruct((n, width), jnp.bfloat16) for n in sizes),
        in_specs=[pl.BlockSpec(memory_space=pltpu.VMEM)] * 3,
        out_specs=(pl.BlockSpec(memory_space=pltpu.VMEM),) * len(sizes),
        scratch_shapes=[pltpu.VMEM((len(sizes), sizes[0], rows), jnp.bfloat16)],
        compiler_params=pltpu.CompilerParams(vmem_limit_bytes=16 * 2**20),
        cost_estimate=pl.CostEstimate(
            flops=2 * rows * sum(sizes) * width,
            bytes_accessed=2 * (rows + sum(sizes)) * width,
            transcendentals=rows,
        ),
    )(resid, gain, places)


def slots_of(routes, experts):
    rows = routes.shape[0]
    ids = jnp.arange(experts, dtype=jnp.int32)
    first = routes[:, 0:1] == ids
    second = routes[:, 1:2] == ids
    named = (first | second).astype(jnp.bfloat16)
    at = jnp.arange(rows, dtype=jnp.int32)
    earlier = (at[:, None] > at[None, :]).astype(jnp.bfloat16)
    rank = dot(earlier, named)
    ranks = [
        jnp.sum(jnp.where(mine, rank, 0.0), axis=1).astype(jnp.int32) for mine in (first, second)
    ]
    return [routes[:, k] for k in range(2)], ranks


def layer(
    conv_in,
    conv_pre,
    conv_post,
    taps,
    out_proj,
    stream,
    norm_gain,
    routes,
    route_weight,
    gate_w,
    up_w,
    down_w,
):
    sp = lax.axis_size("sp")
    tp = lax.axis_size("tp")
    me = lax.axis_index("tp")
    core = lax.axis_index("sp") % 2
    experts = gate_w.shape[0] * sp
    own_rows, width = stream.shape
    channels = conv_in.shape[1]
    lanes = channels // 2

    mine = lax.dynamic_slice_in_dim(out_proj, core * lanes, lanes, axis=0)
    theirs = lax.dynamic_slice_in_dim(out_proj, (1 - core) * lanes, lanes, axis=0)
    after, before = shift(mine, -1), shift(mine, 1)
    half = lanes // 2
    opposite = jnp.concatenate([shift(after[:half], -1), shift(before[half:], 1)])
    proj = [mine, after, opposite, before]
    unit = gate_w.shape[2] // 2
    halves_of = [
        (jnp.concatenate([gate_w[0, :, cut], up_w[0, :, cut]], axis=1), down_w[0, cut])
        for cut in (slice(0, unit), slice(unit, 2 * unit))
    ]

    edge = jnp.stack([conv_in, conv_pre])
    up = [(i, i + 1) for i in range(sp - 1)]
    prior = lax.ppermute(edge[:, -1:], "sp", up)
    later = lax.ppermute(edge[:, :1], "sp", [(j, i) for i, j in up])
    f32 = jnp.float32
    product = conv_pre.astype(f32) * conv_in.astype(f32)
    padded = jnp.concatenate(
        [
            prior[0].astype(f32) * prior[1].astype(f32),
            product,
            later[0].astype(f32) * later[1].astype(f32),
        ]
    )
    convolved = taps[0] * padded[:-2] + taps[1] * padded[1:-1] + taps[2] * padded[2:]
    mixed = (conv_post.astype(f32) * convolved).astype(jnp.bfloat16)
    low, high = mixed[:, :lanes], mixed[:, lanes:]
    mixed = jnp.concatenate(
        [jnp.where(core == 0, low, high), jnp.where(core == 0, high, low)], axis=1
    )

    def rows_for(d):
        return lax.dynamic_slice_in_dim(mixed, ((me - d) % tp) * own_rows, own_rows, axis=0)

    pieces = [rows_for(0)] + [shift(rows_for(d), -d) for d in range(1, tp)]
    low, high = [
        [both(w, pairs) for w in held] for held, pairs in zip(halves_of, weight_routes(tp))
    ]
    other = {d: core_swap(proj[d]) for d in (1, 3)}
    other[2] = core_swap(opposite)
    other[0] = theirs

    def product_of(d):
        return dot(pieces[d][:, :lanes], proj[d]) + dot(pieces[d][:, lanes:], other[d])

    branch = product_of(0) + product_of(1) + product_of(3)
    branch += product_of(2)

    resid = (stream.astype(f32) + branch).astype(jnp.bfloat16)
    expert_of, rank_of = slots_of(routes, experts)

    firsts = [sum(CHUNKS[:at]) for at in range(len(CHUNKS))]
    places = []
    for first, size in zip(firsts, CHUNKS):
        for e, r in zip(expert_of, rank_of):
            inside = (r >= first) & (r < first + size)
            places.append(jnp.where(inside, e * size + r - first, -1))
    filled = fill(resid, norm_gain[None, :], jnp.stack(places), [experts * size for size in CHUNKS])

    def dispatch(rows, size):
        rows = rows.reshape(experts, size, width)
        arrived = lax.all_to_all(rows, "sp", split_axis=0, concat_axis=0, tiled=True)
        return arrived.reshape(experts * size, width)

    routes_in = row_routes(tp)

    def give_back(arrived, size):
        mine_rows = jnp.concatenate([both(arrived, pairs) for pairs in routes_in])
        their_rows = core_swap(mine_rows)
        (their_out,) = ffn(their_rows, low, high)
        met = core_swap(their_out)
        paired = ffn(mine_rows, low, high, met)
        halves = [both(x, flipped(pairs)) for x, pairs in zip(paired, routes_in)]
        out = sum_of(*halves)
        out = out.reshape(experts, size, width)
        returned = lax.all_to_all(out, "sp", split_axis=0, concat_axis=0, tiled=True)
        return returned.reshape(experts * size, width)

    sent = [dispatch(rows, size) for rows, size in zip(filled, CHUNKS)]
    returned = [give_back(arrived, size) for arrived, size in zip(sent, CHUNKS)]
    return combine(resid, *returned, jnp.stack(places, axis=1), route_weight)


def solution(mesh):
    placed = (
        P("sp", "tp"),
        P("sp", "tp"),
        P("sp", "tp"),
        P(None, "tp"),
        P("tp", None),
        P(("sp", "tp"), None),
        P(),
        P(("sp", "tp"), None),
        P(("sp", "tp"), None),
        P("sp", None, "tp"),
        P("sp", None, "tp"),
        P("sp", "tp", None),
    )
    return jax.shard_map(
        layer, mesh=mesh, in_specs=placed, out_specs=P(("sp", "tp"), None), check_vma=False
    )
```

profile of v0, /device:TPU:1, one launch (start us, length us, event | category | flops | bytes accessed | tf_op | source)
XLA Modules:
  0.0 331.9 jit_solution(6946473272156685881)
XLA Ops:
  0.1 1.2 copy-done
  1.3 2.2 collective-permute-start.6
  3.5 1.5 collective-permute-start.3
  5.0 0.7 pad_maximum_fusion.5
  5.7 4.7 %collective-permute-start.1 = (bf16[2,1,256]{2,1,0:T(2,128)(2,1)S(1)}, bf16[2,1,256]{2,1,0:T(2,128)(2,1)S(1)}, u32[]{:S(2)}, u32[]{:S(2)}) collective-permute-start(bf16[2,1,256]{2,1,0:T(2,128)(2,1)S(1)} %get-tuple-element.26), channel_id=1, source_target_pairs={{4,0},{8,4},{12,8},{16,12},{20,16},{24,20},{28,24},{32,28},{36,32}... | collective-permute-start | bytes 3080 | tf_op jit(solution)/shard_map/ppermute | solution.py:285
  10.4 1.9 collective-permute-start
  12.9 0.6 collective-permute-done
  13.5 1.3 fusion.8
  15.0 1.7 collective-permute-start.8
  16.7 1.1 collective-permute-start.2
  18.1 0.4 convolution_add_fusion.3
  18.5 1.0 slice.141
  19.4 0.7 collective-permute-start.9
  20.1 1.0 slice.142
  21.1 0.9 collective-permute-start.10
  22.0 1.5 collective-permute-start.7
  23.5 1.4 fusion.23
  24.9 3.5 %collective-permute-done.9 = bf16[64,2048]{1,0:T(8,128)(2,1)S(1)} collective-permute-done((bf16[64,2048]{1,0:T(8,128)(2,1)S(1)}, bf16[64,2048]{1,0:T(8,128)(2,1)S(1)}, u32[]{:S(2)}, u32[]{:S(2)}) %collective-permute-start.9) | collective-permute-done | bytes 262176 | tf_op jit(solution)/shard_map/ppermute | solution.py:17
  28.4 1.3 collective-permute-start.4
  29.8 1.4 collective-permute-start.11
  31.2 1.4 fusion.26
  33.8 0.7 copy-done.12
  34.5 0.5 fusion.4.resid
  35.0 2.8 shard_map.118
  37.8 0.9 copy-done.2
  38.7 1.2 reshape.272
  39.9 12.7 %all-to-all-start.2 = ((bf16[64,4,2048]{2,1,0:T(4,128)(2,1)}), bf16[64,4,2048]{2,1,0:T(4,128)(2,1)S(1)}, u32[]{:S(2)}, u32[]{:S(2)}) async-start(bf16[64,4,2048]{2,1,0:T(4,128)(2,1)} %reshape.272), calls=%async_computation.2 | async-start | bytes 2097152 | tf_op jit(solution)/shard_map/all_to_all | solution.py:332
  52.6 1.2 reshape.268
  53.8 26.9 %all-to-all-done.2 = bf16[64,4,2048]{2,1,0:T(4,128)(2,1)S(1)} async-done(((bf16[64,4,2048]{2,1,0:T(4,128)(2,1)}), bf16[64,4,2048]{2,1,0:T(4,128)(2,1)S(1)}, u32[]{:S(2)}, u32[]{:S(2)}) %all-to-all-start.2) | async-done | bytes 1048608 | tf_op jit(solution)/shard_map/all_to_all | solution.py:332
  80.8 6.3 %all-to-all-start = ((bf16[64,4,2048]{2,1,0:T(4,128)(2,1)}), bf16[64,4,2048]{2,1,0:T(4,128)(2,1)S(1)}, u32[]{:S(2)}, u32[]{:S(2)}) async-start(bf16[64,4,2048]{2,1,0:T(4,128)(2,1)} %reshape.268), calls=%async_computation | async-start | bytes 2097152 | tf_op jit(solution)/shard_map/all_to_all | solution.py:332
  87.3 1.2 collective-permute-start.22
  88.5 0.9 collective-permute-start.23
  89.4 2.4 slice_bitcast_fusion.2
  91.9 1.5 pad_maximum_fusion
  93.4 1.3 collective-permute-start.14
  94.7 1.5 pad_maximum_fusion.1
  96.3 19.0 %all-to-all-done = bf16[64,4,2048]{2,1,0:T(4,128)(2,1)S(1)} async-done(((bf16[64,4,2048]{2,1,0:T(4,128)(2,1)}), bf16[64,4,2048]{2,1,0:T(4,128)(2,1)S(1)}, u32[]{:S(2)}, u32[]{:S(2)}) %all-to-all-start) | async-done | bytes 1048608 | tf_op jit(solution)/shard_map/all_to_all | solution.py:332
  115.2 1.1 reshape.269
  116.3 1.1 collective-permute-start.12
  117.4 1.6 collective-permute-start.13
  119.0 1.3 constant_dynamic-update-slice_fusion.5
  120.7 35.9 %collective-permute-done.12 = bf16[256,2048]{1,0:T(8,128)(2,1)S(1)} collective-permute-done((bf16[256,2048]{1,0:T(8,128)(2,1)}, bf16[256,2048]{1,0:T(8,128)(2,1)S(1)}, u32[]{:S(2)}, u32[]{:S(2)}) %collective-permute-start.12) | collective-permute-done | bytes 1048608 | tf_op jit(solution)/shard_map/ppermute | solution.py:30
  156.6 3.0 collective-permute-start.16
  159.7 11.6 %collective-permute-done.16.down_low = bf16[256,2048]{1,0:T(8,128)(2,1)S(1)} collective-permute-done((bf16[256,2048]{1,0:T(8,128)(2,1)S(1)}, bf16[256,2048]{1,0:T(8,128)(2,1)S(1)}, u32[]{:S(2)}, u32[]{:S(2)}) %collective-permute-start.16) | collective-permute-done | bytes 1048608 | tf_op jit(solution)/shard_map/ppermute | solution.py:30
  171.3 2.0 collective-permute-start.18
  173.3 10.6 %shard_map.122 = bf16[512,2048]{1,0:T(8,128)(2,1)S(1)} custom-call(bf16[512,2048]{1,0:T(8,128)(2,1)S(1)} %collective-permute-done.24.rows, bf16[2048,512]{1,0:T(8,128)(2,1)} %collective-permute-done.14.gu_low, bf16[2048,512]{1,0:T(8,128)(2,1)} %collective-permute-done.15.gu_high, bf16[256,2048]{1,0:T(8,128)(2,1)S(1)} %collective-permute-done.16.down_low, ...), custom_call_target="tpu_custom_call" | custom-call | flops 3221225472 | bytes 10485760 | tf_op jit(solution)/shard_map/pallas_call | solution.py:119
  184.0 3.2 collective-permute-start.25
  187.2 11.6 %shard_map.119 = bf16[512,2048]{1,0:T(8,128)(2,1)} custom-call(bf16[512,2048]{1,0:T(8,128)(2,1)S(1)} %collective-permute-done.18.rows, bf16[2048,512]{1,0:T(8,128)(2,1)} %collective-permute-done.14.gu_low, bf16[2048,512]{1,0:T(8,128)(2,1)} %collective-permute-done.15.gu_high, bf16[256,2048]{1,0:T(8,128)(2,1)S(1)} %collective-permute-done.16.down_low, ...), custom_call_target="tpu_custom_call" | custom-call | flops 3221225472 | bytes 10485760 | tf_op jit(solution)/shard_map/pallas_call | solution.py:119
  198.8 10.3 %shard_map.123 = (bf16[256,2048]{1,0:T(8,128)(2,1)S(1)}, bf16[256,2048]{1,0:T(8,128)(2,1)S(1)}) custom-call(bf16[512,2048]{1,0:T(8,128)(2,1)S(1)} %constant_dynamic-update-slice_fusion.4.rows, bf16[2048,512]{1,0:T(8,128)(2,1)} %collective-permute-done.14.gu_low, bf16[2048,512]{1,0:T(8,128)(2,1)} %collective-permute-done.15.gu_high, ...), custom_call_target="tpu_custom_call" | custom-call | flops 3221225472 | bytes 10485760 | tf_op jit(solution)/shard_map/pallas_call | solution.py:119
  209.1 0.4 collective-permute-start.26
  209.8 25.5 %collective-permute-done.26.a = bf16[256,2048]{1,0:T(8,128)(2,1)S(1)} collective-permute-done((bf16[256,2048]{1,0:T(8,128)(2,1)S(1)}, bf16[256,2048]{1,0:T(8,128)(2,1)S(1)}, u32[]{:S(2)}, u32[]{:S(2)}) %collective-permute-start.26) | collective-permute-done | bytes 1048608 | tf_op jit(solution)/shard_map/ppermute | solution.py:30
  235.6 1.3 reshape.274
  236.9 10.4 %all-to-all-start.3 = ((bf16[64,4,2048]{2,1,0:T(4,128)(2,1)}), bf16[64,4,2048]{2,1,0:T(4,128)(2,1)}, u32[]{:S(2)}, u32[]{:S(2)}) async-start(bf16[64,4,2048]{2,1,0:T(4,128)(2,1)} %reshape.274), calls=%async_computation.3 | async-start | bytes 2097152 | tf_op jit(solution)/shard_map/all_to_all | solution.py:346
  247.3 1.2 copy-done.7
  248.5 10.9 %shard_map.120 = (bf16[256,2048]{1,0:T(8,128)(2,1)S(1)}, bf16[256,2048]{1,0:T(8,128)(2,1)S(1)}) custom-call(bf16[512,2048]{1,0:T(8,128)(2,1)S(1)} %constant_dynamic-update-slice_fusion.2.rows, bf16[2048,512]{1,0:T(8,128)(2,1)} %collective-permute-done.14.gu_low, bf16[2048,512]{1,0:T(8,128)(2,1)} %collective-permute-done.15.gu_high, ...), custom_call_target="tpu_custom_call" | custom-call | flops 3221225472 | bytes 10485760 | tf_op jit(solution)/shard_map/pallas_call | solution.py:119
  259.4 1.4 collective-permute-start.20
  260.8 24.3 %collective-permute-done.20.a = bf16[256,2048]{1,0:T(8,128)(2,1)S(1)} collective-permute-done((bf16[256,2048]{1,0:T(8,128)(2,1)S(1)}, bf16[256,2048]{1,0:T(8,128)(2,1)S(1)}, u32[]{:S(2)}, u32[]{:S(2)}) %collective-permute-start.20) | collective-permute-done | bytes 1048608 | tf_op jit(solution)/shard_map/ppermute | solution.py:30
  285.5 1.2 reshape.270
  286.7 11.2 %all-to-all-start.1 = ((bf16[64,4,2048]{2,1,0:T(4,128)(2,1)}), bf16[64,4,2048]{2,1,0:T(4,128)(2,1)}, u32[]{:S(2)}, u32[]{:S(2)}) async-start(bf16[64,4,2048]{2,1,0:T(4,128)(2,1)} %reshape.270), calls=%async_computation.1 | async-start | bytes 2097152 | tf_op jit(solution)/shard_map/all_to_all | solution.py:346
  298.2 1.3 reshape.275.second
  299.6 26.4 %all-to-all-done.1 = bf16[64,4,2048]{2,1,0:T(4,128)(2,1)} async-done(((bf16[64,4,2048]{2,1,0:T(4,128)(2,1)}), bf16[64,4,2048]{2,1,0:T(4,128)(2,1)}, u32[]{:S(2)}, u32[]{:S(2)}) %all-to-all-start.1) | async-done | bytes 1048608 | tf_op jit(solution)/shard_map/all_to_all | solution.py:346
  326.0 1.4 reshape.271.first
  327.5 1.1 copy-done.3
  328.6 3.3 %shard_map.125 = bf16[192,2048]{1,0:T(8,128)(2,1)} custom-call(bf16[192,2048]{1,0:T(8,128)(2,1)S(1)} %copy-done.3, bf16[256,2048]{1,0:T(8,128)(2,1)S(1)} %reshape.271.first, bf16[256,2048]{1,0:T(8,128)(2,1)S(1)} %reshape.275.second, s32[192,4]{1,0:T(8,128)S(1)} %copy.29.places, f32[192,2]{1,0:T(8,128)S(1)} %copy.30.weight), custom_call_target="tpu_custom_call" | custom-call | flops 805306368 | bytes 3670016 | tf_op jit(solution)/shard_map/pallas_call | solution.py:176
  (87 shorter events, 3.9 us)
Async XLA Ops:
  0.0 1.2 copy-start
  0.0 12.4 %copy-start.11 = (bf16[768,256]{1,0:T(8,128)(2,1)S(1)}, bf16[768,256]{1,0:T(8,128)(2,1)}, u32[]{:S(2)}) copy-start(bf16[768,256]{1,0:T(8,128)(2,1)} %param.12) | copy-start | bytes 1179652
  0.0 12.4 %copy-start.10 = (bf16[768,256]{1,0:T(8,128)(2,1)S(1)}, bf16[768,256]{1,0:T(8,128)(2,1)}, u32[]{:S(2)}) copy-start(bf16[768,256]{1,0:T(8,128)(2,1)} %param.13) | copy-start | bytes 1179652
  0.0 12.5 %copy-start.14 = (f32[3,256]{1,0:T(4,128)S(1)}, f32[3,256]{1,0:T(4,128)}, u32[]{:S(2)}) copy-start(f32[3,256]{1,0:T(4,128)} %param.15) | copy-start | bytes 9220
  0.0 12.5 %copy-start.13 = (s32[192,2]{0,1:T(2,128)S(1)}, s32[192,2]{0,1:T(2,128)}, u32[]{:S(2)}) copy-start(s32[192,2]{0,1:T(2,128)} %param.19) | copy-start | bytes 4612
  1.3 18.8 %collective-permute-start.6 = (bf16[128,2048]{1,0:T(8,128)(2,1)S(1)}, bf16[128,2048]{1,0:T(8,128)(2,1)}, u32[]{:S(2)}, u32[]{:S(2)}) collective-permute-start(bf16[128,2048]{1,0:T(8,128)(2,1)S(1)} %constant_dynamic-slice_fusion), channel_id=1, source_target_pairs={{0,1},{1,2},{2,3},{3,0},{4,5},{5,6},{6,7},{7,4},{8,9},{9,10},{10,1... | collective-permute-start | bytes 1572872 | tf_op jit(solution)/shard_map/ppermute | solution.py:17
  3.5 15.0 %collective-permute-start.3 = (bf16[128,2048]{1,0:T(8,128)(2,1)S(1)}, bf16[128,2048]{1,0:T(8,128)(2,1)}, u32[]{:S(2)}, u32[]{:S(2)}) collective-permute-start(bf16[128,2048]{1,0:T(8,128)(2,1)S(1)} %constant_dynamic-slice_fusion), channel_id=1, source_target_pairs={{0,3},{1,0},{2,1},{3,2},{4,7},{5,4},{6,5},{7,6},{8,11},{9,8},{10,9... | collective-permute-start | bytes 1572872 | tf_op jit(solution)/shard_map/ppermute | solution.py:17
  5.7 7.2 %collective-permute-start.1 = (bf16[2,1,256]{2,1,0:T(2,128)(2,1)S(1)}, bf16[2,1,256]{2,1,0:T(2,128)(2,1)S(1)}, u32[]{:S(2)}, u32[]{:S(2)}) collective-permute-start(bf16[2,1,256]{2,1,0:T(2,128)(2,1)S(1)} %get-tuple-element.26), channel_id=1, source_target_pairs={{4,0},{8,4},{12,8},{16,12},{20,16},{24,20},{28,24},{32,28},{36,32}... | collective-permute-start | bytes 3080 | tf_op jit(solution)/shard_map/ppermute | solution.py:285
  10.4 3.1 collective-permute-start
  14.9 7.1 %collective-permute-start.5 = (bf16[192,256]{1,0:T(8,128)(2,1)S(1)}, bf16[192,256]{1,0:T(8,128)(2,1)S(1)}, u32[]{:S(2)}, u32[]{:S(2)}) collective-permute-start(bf16[192,256]{1,0:T(8,128)(2,1)S(1)} %get-tuple-element.29), channel_id=1, source_target_pairs={{0,1},{1,2},{2,3},{3,0},{4,5},{5,6},{6,7},{7,4},{8,9},{9,10},{10,1... | collective-permute-start | bytes 294920 | tf_op jit(solution)/shard_map/ppermute | solution.py:17
  15.0 18.0 %collective-permute-start.8 = (bf16[192,256]{1,0:T(8,128)(2,1)S(1)}, bf16[192,256]{1,0:T(8,128)(2,1)S(1)}, u32[]{:S(2)}, u32[]{:S(2)}) collective-permute-start(bf16[192,256]{1,0:T(8,128)(2,1)S(1)} %get-tuple-element.30), channel_id=1, source_target_pairs={{0,2},{1,3},{2,0},{3,1},{4,6},{5,7},{6,4},{7,5},{8,10},{9,11},{10,... | collective-permute-start | bytes 294920 | tf_op jit(solution)/shard_map/ppermute | solution.py:17
  16.7 14.6 %collective-permute-start.2 = (bf16[192,256]{1,0:T(8,128)(2,1)S(1)}, bf16[192,256]{1,0:T(8,128)(2,1)S(1)}, u32[]{:S(2)}, u32[]{:S(2)}) collective-permute-start(bf16[192,256]{1,0:T(8,128)(2,1)S(1)} %get-tuple-element.27), channel_id=1, source_target_pairs={{0,3},{1,0},{2,1},{3,2},{4,7},{5,4},{6,5},{7,6},{8,11},{9,8},{10,9... | collective-permute-start | bytes 294920 | tf_op jit(solution)/shard_map/ppermute | solution.py:17
  19.4 9.0 %collective-permute-start.9 = (bf16[64,2048]{1,0:T(8,128)(2,1)S(1)}, bf16[64,2048]{1,0:T(8,128)(2,1)S(1)}, u32[]{:S(2)}, u32[]{:S(2)}) collective-permute-start(bf16[64,2048]{1,0:T(8,128)(2,1)S(1)} %slice.141), channel_id=1, source_target_pairs={{0,3},{1,0},{2,1},{3,2},{4,7},{5,4},{6,5},{7,6},{8,11},{9,8},{10,9... | collective-permute-start | bytes 786440 | tf_op jit(solution)/shard_map/ppermute | solution.py:17
  21.1 8.7 %collective-permute-start.10 = (bf16[64,2048]{1,0:T(8,128)(2,1)S(1)}, bf16[64,2048]{1,0:T(8,128)(2,1)S(1)}, u32[]{:S(2)}, u32[]{:S(2)}) collective-permute-start(bf16[64,2048]{1,0:T(8,128)(2,1)S(1)} %slice.142), channel_id=1, source_target_pairs={{0,1},{1,2},{2,3},{3,0},{4,5},{5,6},{6,7},{7,4},{8,9},{9,10},{10,1... | collective-permute-start | bytes 786440 | tf_op jit(solution)/shard_map/ppermute | solution.py:17
  22.0 10.6 %collective-permute-start.7 = (bf16[128,2048]{1,0:T(8,128)(2,1)}, bf16[128,2048]{1,0:T(8,128)(2,1)S(1)}, u32[]{:S(2)}, u32[]{:S(2)}) collective-permute-start(bf16[128,2048]{1,0:T(8,128)(2,1)} %collective-permute-done.6), channel_id=1, source_target_pairs={{0,4},{4,0},{8,12},{12,8},{16,20},{20,16},{24,28},{28,24},{32,36},... | collective-permute-start | bytes 1572872 | tf_op jit(solution)/shard_map/ppermute | solution.py:21
  28.4 5.3 %collective-permute-start.4 = (bf16[128,2048]{1,0:T(8,128)(2,1)}, bf16[128,2048]{1,0:T(8,128)(2,1)S(1)}, u32[]{:S(2)}, u32[]{:S(2)}) collective-permute-start(bf16[128,2048]{1,0:T(8,128)(2,1)} %collective-permute-done.3), channel_id=1, source_target_pairs={{0,4},{4,0},{8,12},{12,8},{16,20},{20,16},{24,28},{28,24},{32,36},... | collective-permute-start | bytes 1572872 | tf_op jit(solution)/shard_map/ppermute | solution.py:21
  29.8 3.2 collective-permute-start.11
  33.4 1.1 copy-start.12
  33.7 1.3 copy-start.8
  37.8 0.9 copy-start.2
  39.9 40.9 %all-to-all-start.2 = ((bf16[64,4,2048]{2,1,0:T(4,128)(2,1)}), bf16[64,4,2048]{2,1,0:T(4,128)(2,1)S(1)}, u32[]{:S(2)}, u32[]{:S(2)}) async-start(bf16[64,4,2048]{2,1,0:T(4,128)(2,1)} %reshape.272), calls=%async_computation.2 | async-start | bytes 2097152 | tf_op jit(solution)/shard_map/all_to_all | solution.py:332
  80.8 34.4 %all-to-all-start = ((bf16[64,4,2048]{2,1,0:T(4,128)(2,1)}), bf16[64,4,2048]{2,1,0:T(4,128)(2,1)S(1)}, u32[]{:S(2)}, u32[]{:S(2)}) async-start(bf16[64,4,2048]{2,1,0:T(4,128)(2,1)} %reshape.268), calls=%async_computation | async-start | bytes 2097152 | tf_op jit(solution)/shard_map/all_to_all | solution.py:332
  87.3 30.1 %collective-permute-start.22 = (bf16[256,2048]{1,0:T(8,128)(2,1)S(1)}, bf16[256,2048]{1,0:T(8,128)(2,1)}, u32[]{:S(2)}, u32[]{:S(2)}) collective-permute-start(bf16[256,2048]{1,0:T(8,128)(2,1)S(1)} %reshape.273), channel_id=1, source_target_pairs={{4,7},{1,0},{6,5},{3,2},{0,6},{5,3},{2,4},{7,1},{12,15},{9,8},{14,... | collective-permute-start | bytes 3145736 | tf_op jit(solution)/shard_map/ppermute | solution.py:30
  88.5 31.8 %collective-permute-start.23 = (bf16[256,2048]{1,0:T(8,128)(2,1)S(1)}, bf16[256,2048]{1,0:T(8,128)(2,1)S(1)}, u32[]{:S(2)}, u32[]{:S(2)}) collective-permute-start(bf16[256,2048]{1,0:T(8,128)(2,1)S(1)} %reshape.273), channel_id=1, source_target_pairs={{4,5},{1,2},{6,7},{3,0},{0,4},{5,1},{2,6},{7,3},{12,13},{9,10},{14... | collective-permute-start | bytes 3145736 | tf_op jit(solution)/shard_map/ppermute | solution.py:30
  93.4 79.9 %collective-permute-start.14 = (bf16[2048,512]{1,0:T(8,128)(2,1)}, bf16[2048,512]{1,0:T(8,128)(2,1)}, u32[]{:S(2)}, u32[]{:S(2)}) collective-permute-start(bf16[2048,512]{1,0:T(8,128)(2,1)} %pad_maximum_fusion), channel_id=1, source_target_pairs={{0,4},{5,1},{2,6},{7,3},{4,7},{1,0},{6,5},{3,2},{8,12},{13,9},{10,... | collective-permute-start | bytes 6291464 | tf_op jit(solution)/shard_map/ppermute | solution.py:30
  96.2 77.1 %collective-permute-start.15 = (bf16[2048,512]{1,0:T(8,128)(2,1)}, bf16[2048,512]{1,0:T(8,128)(2,1)}, u32[]{:S(2)}, u32[]{:S(2)}) collective-permute-start(bf16[2048,512]{1,0:T(8,128)(2,1)} %pad_maximum_fusion.1), channel_id=1, source_target_pairs={{0,4},{5,1},{2,6},{7,3},{4,5},{1,2},{6,7},{3,0},{8,12},{13,9},{10,... | collective-permute-start | bytes 6291464 | tf_op jit(solution)/shard_map/ppermute | solution.py:30
  116.3 4.2 %copy-start.9 = (bf16[1,512,2048]{2,1,0:T(8,128)(2,1)S(1)}, bf16[1,512,2048]{2,1,0:T(8,128)(2,1)}, u32[]{:S(2)}) copy-start(bf16[1,512,2048]{2,1,0:T(8,128)(2,1)} %param.23) | copy-start | bytes 6291460
  116.3 40.2 %collective-permute-start.12 = (bf16[256,2048]{1,0:T(8,128)(2,1)}, bf16[256,2048]{1,0:T(8,128)(2,1)S(1)}, u32[]{:S(2)}, u32[]{:S(2)}) collective-permute-start(bf16[256,2048]{1,0:T(8,128)(2,1)} %reshape.269), channel_id=1, source_target_pairs={{4,7},{1,0},{6,5},{3,2},{0,6},{5,3},{2,4},{7,1},{12,15},{9,8},{14,... | collective-permute-start | bytes 3145736 | tf_op jit(solution)/shard_map/ppermute | solution.py:30
  117.4 42.2 %collective-permute-start.13 = (bf16[256,2048]{1,0:T(8,128)(2,1)}, bf16[256,2048]{1,0:T(8,128)(2,1)S(1)}, u32[]{:S(2)}, u32[]{:S(2)}) collective-permute-start(bf16[256,2048]{1,0:T(8,128)(2,1)} %reshape.269), channel_id=1, source_target_pairs={{4,5},{1,2},{6,7},{3,0},{0,4},{5,1},{2,6},{7,3},{12,13},{9,10},{14... | collective-permute-start | bytes 3145736 | tf_op jit(solution)/shard_map/ppermute | solution.py:30
  120.4 52.9 %collective-permute-start.24 = (bf16[512,2048]{1,0:T(8,128)(2,1)S(1)}, bf16[512,2048]{1,0:T(8,128)(2,1)S(1)}, u32[]{:S(2)}, u32[]{:S(2)}) collective-permute-start(bf16[512,2048]{1,0:T(8,128)(2,1)S(1)} %constant_dynamic-update-slice_fusion.4.rows), channel_id=1, source_target_pairs={{0,4},{4,0},{8,12},{12,8},{16,20},{20,16},{24,28},{28,24},{32,36},... | collective-permute-start | bytes 6291464 | tf_op jit(solution)/shard_map/ppermute | solution.py:21
  156.6 14.8 %collective-permute-start.16 = (bf16[256,2048]{1,0:T(8,128)(2,1)S(1)}, bf16[256,2048]{1,0:T(8,128)(2,1)S(1)}, u32[]{:S(2)}, u32[]{:S(2)}) collective-permute-start(bf16[256,2048]{1,0:T(8,128)(2,1)S(1)} %get-tuple-element.20), channel_id=1, source_target_pairs={{0,4},{5,1},{2,6},{7,3},{4,7},{1,0},{6,5},{3,2},{8,12},{13,9},{10,... | collective-permute-start | bytes 3145736 | tf_op jit(solution)/shard_map/ppermute | solution.py:30
  159.6 13.7 %collective-permute-start.17 = (bf16[256,2048]{1,0:T(8,128)(2,1)S(1)}, bf16[256,2048]{1,0:T(8,128)(2,1)S(1)}, u32[]{:S(2)}, u32[]{:S(2)}) collective-permute-start(bf16[256,2048]{1,0:T(8,128)(2,1)S(1)} %get-tuple-element.19), channel_id=1, source_target_pairs={{0,4},{5,1},{2,6},{7,3},{4,5},{1,2},{6,7},{3,0},{8,12},{13,9},{10,... | collective-permute-start | bytes 3145736 | tf_op jit(solution)/shard_map/ppermute | solution.py:30
  171.3 27.5 %copy-start.4 = (bf16[256,2048]{1,0:T(8,128)(2,1)}, bf16[256,2048]{1,0:T(8,128)(2,1)S(1)}, u32[]{:S(2)}) copy-start(bf16[256,2048]{1,0:T(8,128)(2,1)S(1)} %collective-permute-done.16.down_low) | copy-start | bytes 3145732
  171.3 15.9 %collective-permute-start.18 = (bf16[512,2048]{1,0:T(8,128)(2,1)S(1)}, bf16[512,2048]{1,0:T(8,128)(2,1)S(1)}, u32[]{:S(2)}, u32[]{:S(2)}) collective-permute-start(bf16[512,2048]{1,0:T(8,128)(2,1)S(1)} %constant_dynamic-update-slice_fusion.2.rows), channel_id=1, source_target_pairs={{0,4},{4,0},{8,12},{12,8},{16,20},{20,16},{24,28},{28,24},{32,36},... | collective-permute-start | bytes 6291464 | tf_op jit(solution)/shard_map/ppermute | solution.py:21
  173.3 25.5 %copy-start.6 = (bf16[256,2048]{1,0:T(8,128)(2,1)}, bf16[256,2048]{1,0:T(8,128)(2,1)S(1)}, u32[]{:S(2)}) copy-start(bf16[256,2048]{1,0:T(8,128)(2,1)S(1)} %collective-permute-done.17.down_high) | copy-start | bytes 3145732
  184.0 14.9 %collective-permute-start.25 = (bf16[512,2048]{1,0:T(8,128)(2,1)S(1)}, bf16[512,2048]{1,0:T(8,128)(2,1)S(1)}, u32[]{:S(2)}, u32[]{:S(2)}) collective-permute-start(bf16[512,2048]{1,0:T(8,128)(2,1)S(1)} %shard_map.122), channel_id=1, source_target_pairs={{0,4},{4,0},{8,12},{12,8},{16,20},{20,16},{24,28},{28,24},{32,36},... | collective-permute-start | bytes 6291464 | tf_op jit(solution)/shard_map/ppermute | solution.py:21
  198.8 48.4 %collective-permute-start.19 = (bf16[512,2048]{1,0:T(8,128)(2,1)}, bf16[512,2048]{1,0:T(8,128)(2,1)}, u32[]{:S(2)}, u32[]{:S(2)}) collective-permute-start(bf16[512,2048]{1,0:T(8,128)(2,1)} %shard_map.119), channel_id=1, source_target_pairs={{0,4},{4,0},{8,12},{12,8},{16,20},{20,16},{24,28},{28,24},{32,36},... | collective-permute-start | bytes 6291464 | tf_op jit(solution)/shard_map/ppermute | solution.py:21
  209.1 26.2 %collective-permute-start.26 = (bf16[256,2048]{1,0:T(8,128)(2,1)S(1)}, bf16[256,2048]{1,0:T(8,128)(2,1)S(1)}, u32[]{:S(2)}, u32[]{:S(2)}) collective-permute-start(bf16[256,2048]{1,0:T(8,128)(2,1)S(1)} %get-tuple-element.15), channel_id=1, source_target_pairs={{7,4},{0,1},{5,6},{2,3},{6,0},{3,5},{4,2},{1,7},{15,12},{8,9},{13,... | collective-permute-start | bytes 3145736 | tf_op jit(solution)/shard_map/ppermute | solution.py:30
  209.6 25.7 %collective-permute-start.27 = (bf16[256,2048]{1,0:T(8,128)(2,1)S(1)}, bf16[256,2048]{1,0:T(8,128)(2,1)S(1)}, u32[]{:S(2)}, u32[]{:S(2)}) collective-permute-start(bf16[256,2048]{1,0:T(8,128)(2,1)S(1)} %get-tuple-element.16), channel_id=1, source_target_pairs={{5,4},{2,1},{7,6},{0,3},{4,0},{1,5},{6,2},{3,7},{13,12},{10,9},{15... | collective-permute-start | bytes 3145736 | tf_op jit(solution)/shard_map/ppermute | solution.py:30
  236.8 10.4 %copy-start.5 = (bf16[256,2048]{1,0:T(8,128)(2,1)S(1)}, bf16[256,2048]{1,0:T(8,128)(2,1)}, u32[]{:S(2)}) copy-start(bf16[256,2048]{1,0:T(8,128)(2,1)} %copy-done.4) | copy-start | bytes 3145732
  236.9 49.9 %all-to-all-start.3 = ((bf16[64,4,2048]{2,1,0:T(4,128)(2,1)}), bf16[64,4,2048]{2,1,0:T(4,128)(2,1)}, u32[]{:S(2)}, u32[]{:S(2)}) async-start(bf16[64,4,2048]{2,1,0:T(4,128)(2,1)} %reshape.274), calls=%async_computation.3 | async-start | bytes 2097152 | tf_op jit(solution)/shard_map/all_to_all | solution.py:346
  247.3 1.2 copy-start.7
  259.4 25.8 %collective-permute-start.20 = (bf16[256,2048]{1,0:T(8,128)(2,1)S(1)}, bf16[256,2048]{1,0:T(8,128)(2,1)S(1)}, u32[]{:S(2)}, u32[]{:S(2)}) collective-permute-start(bf16[256,2048]{1,0:T(8,128)(2,1)S(1)} %get-tuple-element.12), channel_id=1, source_target_pairs={{7,4},{0,1},{5,6},{2,3},{6,0},{3,5},{4,2},{1,7},{15,12},{8,9},{13,... | collective-permute-start | bytes 3145736 | tf_op jit(solution)/shard_map/ppermute | solution.py:30
  260.8 24.3 %collective-permute-start.21 = (bf16[256,2048]{1,0:T(8,128)(2,1)S(1)}, bf16[256,2048]{1,0:T(8,128)(2,1)S(1)}, u32[]{:S(2)}, u32[]{:S(2)}) collective-permute-start(bf16[256,2048]{1,0:T(8,128)(2,1)S(1)} %get-tuple-element.13), channel_id=1, source_target_pairs={{5,4},{2,1},{7,6},{0,3},{4,0},{1,5},{6,2},{3,7},{13,12},{10,9},{15... | collective-permute-start | bytes 3145736 | tf_op jit(solution)/shard_map/ppermute | solution.py:30
  285.5 12.6 %copy-start.15 = (f32[192,2]{0,1:T(2,128)S(1)}, f32[192,2]{0,1:T(2,128)}, u32[]{:S(2)}) copy-start(f32[192,2]{0,1:T(2,128)} %param.20) | copy-start | bytes 4612
  286.7 39.3 %all-to-all-start.1 = ((bf16[64,4,2048]{2,1,0:T(4,128)(2,1)}), bf16[64,4,2048]{2,1,0:T(4,128)(2,1)}, u32[]{:S(2)}, u32[]{:S(2)}) async-start(bf16[64,4,2048]{2,1,0:T(4,128)(2,1)} %reshape.270), calls=%async_computation.1 | async-start | bytes 2097152 | tf_op jit(solution)/shard_map/all_to_all | solution.py:346
  326.0 5.9 %copy-start.1 = (bf16[256,2048]{1,0:T(8,128)(2,1)S(1)}, bf16[256,2048]{1,0:T(8,128)(2,1)}, u32[]{:S(2)}) copy-start(bf16[256,2048]{1,0:T(8,128)(2,1)} %param.16) | copy-start | bytes 3145732
  327.5 1.1 copy-start.3
where the time goes:
time: 333 us; the launch traced here: 332 us
  waiting for transfers between devices  174 us (52%)
  starting transfers between devices  76.1 us (23%)
  Pallas kernels  50.1 us (15%)
  local copies, waits for them, and re-layouts  20.6 us (6%)
  other arithmetic  5.33 us (2%)
  matrix products  5.24 us (2%)
    ppermute x12, waiting for transfers between devices, both(): return lax.ppermute(x, ('sp', 'tp'), every)  97.3 us
    all_to_all x2, waiting for transfers between devices, dispatch(): lax.all_to_all(rows, 'sp', split_axis=0, concat_axis=0, tiled=True)  45.9 us
    pallas_call x4, Pallas kernels, ffn(): pl.pallas_call(ffn_kernel, out_shape=(shape,) * count, in_specs=[pl.Block...  43.4 us
    all_to_all x2, waiting for transfers between devices, give_back(): lax.all_to_all(out, 'sp', split_axis=0, concat_axis=0, tiled=True)  26.4 us
    all_to_all x2, starting transfers between devices, give_back(): lax.all_to_all(out, 'sp', split_axis=0, concat_axis=0, tiled=True)  21.6 us
    all_to_all x2, starting transfers between devices, dispatch(): lax.all_to_all(rows, 'sp', split_axis=0, concat_axis=0, tiled=True)  19 us
    ppermute x12, starting transfers between devices, both(): return lax.ppermute(x, ('sp', 'tp'), every)  11.2 us
    ppermute x7, starting transfers between devices, core_swap(): lax.ppermute(x, 'sp', [(i, i ^ 1) for i in range(lax.axis_size('sp'))])  9.51 us
  transfers between devices with their start and end apart: 32, of which 9 were waited for; matrix products, arithmetic and copies ran while one was open for 7% of the time, Pallas kernels for 13%

commit v1 on v0

--- a/solution.py
+++ b/solution.py
@@ -68,6 +68,8 @@
 
 
 BLOCK = 256
+DEPTH = 512
+COLUMNS = 512
 
 
 def blocks(length, size):
@@ -79,12 +81,9 @@
     return over
 
 
-def ffn_kernel(rows, gu_low, gu_high, down_low, down_high, *rest):
-    *rest, pre, active = rest
-    met, outs = (rest[0], rest[1:]) if len(rest) == 3 else (None, rest)
+def ffn_kernel(rows, gu_low, gu_high, down_low, down_high, out, pre, active):
     count, width = rows.shape
     unit = down_low.shape[0]
-    each = count // len(outs)
 
     for k, gu in enumerate((gu_low, gu_high)):
 
@@ -92,7 +91,7 @@
         def _(at):
             pre[at, :] = jnp.zeros((at.size, 2 * unit), jnp.float32)
 
-        @blocks(width, BLOCK)
+        @blocks(width, DEPTH)
         def _(at):
             pre[...] += dot(rows[:, at], gu[at, :])
 
@@ -100,27 +99,21 @@
         def _(at):
             active[k, at, :] = clamped_unit(pre[at, :unit], pre[at, unit:]).astype(jnp.bfloat16)
 
-    @blocks(width, BLOCK)
+    @blocks(width, COLUMNS)
     def _(at):
         total = dot(active[0], down_low[:, at]) + dot(active[1], down_high[:, at])
-        if met is not None:
-            total = total + met[:, at].astype(jnp.float32)
-        total = total.astype(jnp.bfloat16)
-        for k, out in enumerate(outs):
-            out[:, at] = total[k * each : (k + 1) * each]
-
-
-def ffn(rows, low, high, met=None):
+        out[:, at] = total.astype(out.dtype)
+
+
+def ffn(rows, low, high):
     number, width = rows.shape
     unit = low[1].shape[0]
-    count = 1 if met is None else 2
-    shape = jax.ShapeDtypeStruct((number // count, width), jnp.bfloat16)
-    operands = (rows, low[0], high[0], low[1], high[1]) + (() if met is None else (met,))
+    shape = jax.ShapeDtypeStruct((number, width), jnp.bfloat16)
     return pl.pallas_call(
         ffn_kernel,
-        out_shape=(shape,) * count,
-        in_specs=[pl.BlockSpec(memory_space=pltpu.VMEM)] * len(operands),
-        out_specs=(pl.BlockSpec(memory_space=pltpu.VMEM),) * count,
+        out_shape=(shape,),
+        in_specs=[pl.BlockSpec(memory_space=pltpu.VMEM)] * 5,
+        out_specs=(pl.BlockSpec(memory_space=pltpu.VMEM),),
         scratch_shapes=[
             pltpu.VMEM((number, 2 * unit), jnp.float32),
             pltpu.VMEM((2, number, unit), jnp.bfloat16),
@@ -131,22 +124,27 @@
             bytes_accessed=4 * number * width + 12 * unit * width,
             transcendentals=2 * number * unit,
         ),
-    )(*operands)
-
-
-def sum_kernel(a, b, out):
-    @blocks(a.shape[0], 32)
-    def _(at):
-        total = a[at, :].astype(jnp.float32) + b[at, :].astype(jnp.float32)
-        out[at, :] = total.astype(out.dtype)
-
-
-def sum_of(a, b):
+    )(rows, low[0], high[0], low[1], high[1])
+
+
+def sum_kernel(a, b, *outs):
+    each = outs[0].shape[0]
+    for k, out in enumerate(outs):
+
+        @blocks(each, 32)
+        def _(at):
+            of = pl.ds(k * each + at.start, at.size)
+            total = a[of, :].astype(jnp.float32) + b[of, :].astype(jnp.float32)
+            out[at, :] = total.astype(out.dtype)
+
+
+def sum_of(a, b, count=1):
+    shape = jax.ShapeDtypeStruct((a.shape[0] // count, a.shape[1]), a.dtype)
     return pl.pallas_call(
         sum_kernel,
-        out_shape=jax.ShapeDtypeStruct(a.shape, a.dtype),
+        out_shape=(shape,) * count,
         in_specs=[pl.BlockSpec(memory_space=pltpu.VMEM)] * 2,
-        out_specs=pl.BlockSpec(memory_space=pltpu.VMEM),
+        out_specs=(pl.BlockSpec(memory_space=pltpu.VMEM),) * count,
         compiler_params=pltpu.CompilerParams(vmem_limit_bytes=8 * 2**20),
         cost_estimate=pl.CostEstimate(
             flops=a.size, bytes_accessed=3 * 2 * a.size, transcendentals=0
@@ -339,9 +337,10 @@
         their_rows = core_swap(mine_rows)
         (their_out,) = ffn(their_rows, low, high)
         met = core_swap(their_out)
-        paired = ffn(mine_rows, low, high, met)
+        (my_out,) = ffn(mine_rows, low, high)
+        paired = sum_of(my_out, met, 2)
         halves = [both(x, flipped(pairs)) for x, pairs in zip(paired, routes_in)]
-        out = sum_of(*halves)
+        (out,) = sum_of(*halves)
         out = out.reshape(experts, size, width)
         returned = lax.all_to_all(out, "sp", split_axis=0, concat_axis=0, tiled=True)
         return returned.reshape(experts * size, width)

time: 333 us -> 330 us (level)
  Pallas kernels: 50.1 us -> 40.7 us
  local copies, waits for them, and re-layouts: 20.6 us -> 27.7 us
    pallas_call x6 -> x8, Pallas kernels: 44 us -> 34.7 us  [the longest x4 33 us: ffn(): pl.pallas_call(ffn_kernel, out_shape=(shape,), in_specs=[pl.BlockSpec(mem...]
    unnamed x36 -> x48, local copies, waits for them, and re-layouts: 6.72 us -> 11.5 us
  transfers between devices with their start and end apart: 32 -> 32, of which waited for: 9 -> 8; matrix products, arithmetic and copies ran while one was open for 7% -> 8% of each run, Pallas kernels for 13% -> 11%
where the time goes in v1:
time: 330 us; the launch traced here: 329 us
  waiting for transfers between devices  171 us (52%)
  starting transfers between devices  76.6 us (23%)
  Pallas kernels  40.7 us (12%)
  local copies, waits for them, and re-layouts  27.7 us (8%)
  other arithmetic  6.29 us (2%)
  matrix products  5.4 us (2%)
    ppermute x12, waiting for transfers between devices, both(): return lax.ppermute(x, ('sp', 'tp'), every)  97 us
    all_to_all x2, waiting for transfers between devices, dispatch(): lax.all_to_all(rows, 'sp', split_axis=0, concat_axis=0, tiled=True)  45.1 us
    pallas_call x4, Pallas kernels, ffn(): pl.pallas_call(ffn_kernel, out_shape=(shape,), in_specs=[pl.BlockSpec(mem...  33 us
    all_to_all x2, waiting for transfers between devices, give_back(): lax.all_to_all(out, 'sp', split_axis=0, concat_axis=0, tiled=True)  26.4 us
    all_to_all x2, starting transfers between devices, give_back(): lax.all_to_all(out, 'sp', split_axis=0, concat_axis=0, tiled=True)  21.7 us
    all_to_all x2, starting transfers between devices, dispatch(): lax.all_to_all(rows, 'sp', split_axis=0, concat_axis=0, tiled=True)  19 us
    unnamed x48, local copies, waits for them, and re-layouts  11.5 us
    ppermute x12, starting transfers between devices, both(): return lax.ppermute(x, ('sp', 'tp'), every)  11.2 us
  transfers between devices with their start and end apart: 32, of which 8 were waited for; matrix products, arithmetic and copies ran while one was open for 8% of the time, Pallas kernels for 11%

profile of v1, /device:TPU:1, one launch (start us, length us, event | category | flops | bytes accessed | tf_op | source)
XLA Modules:
  0.0 328.9 jit_solution(1970817863566041424)
XLA Ops:
  0.1 1.2 copy-done
  1.3 2.2 collective-permute-start.6
  3.5 1.5 collective-permute-start.3
  5.0 1.3 pad_maximum_fusion.5
  6.3 4.7 %collective-permute-start.1 = (bf16[2,1,256]{2,1,0:T(2,128)(2,1)}, bf16[2,1,256]{2,1,0:T(2,128)(2,1)}, u32[]{:S(2)}, u32[]{:S(2)}) collective-permute-start(bf16[2,1,256]{2,1,0:T(2,128)(2,1)} %get-tuple-element.26), channel_id=1, source_target_pairs={{4,0},{8,4},{12,8},{16,12},{20,16},{24,20},{28,24},{32,28},{36,32}... | collective-permute-start | bytes 3080 | tf_op jit(solution)/shard_map/ppermute | solution.py:283
  11.0 1.9 collective-permute-start
  13.5 0.7 fusion.35
  15.4 2.1 collective-permute-start.8
  17.4 1.1 collective-permute-start.2
  19.2 1.0 slice.141
  20.5 1.0 slice.142
  21.5 1.3 collective-permute-start.10
  22.8 1.6 collective-permute-start.7
  24.4 1.4 fusion.23
  25.8 2.8 collective-permute-done.9
  28.6 1.5 collective-permute-start.4
  30.2 1.4 collective-permute-start.11
  31.6 1.4 fusion.26
  34.2 0.7 copy-done.17
  35.6 2.8 shard_map.118
  38.4 0.9 copy-done.2
  39.2 1.2 reshape.272
  40.4 12.7 %all-to-all-start.2 = ((bf16[64,4,2048]{2,1,0:T(4,128)(2,1)}), bf16[64,4,2048]{2,1,0:T(4,128)(2,1)S(1)}, u32[]{:S(2)}, u32[]{:S(2)}) async-start(bf16[64,4,2048]{2,1,0:T(4,128)(2,1)} %reshape.272), calls=%async_computation.2 | async-start | bytes 2097152 | tf_op jit(solution)/shard_map/all_to_all | solution.py:330
  53.1 1.3 reshape.268
  54.4 26.9 %all-to-all-done.2 = bf16[64,4,2048]{2,1,0:T(4,128)(2,1)S(1)} async-done(((bf16[64,4,2048]{2,1,0:T(4,128)(2,1)}), bf16[64,4,2048]{2,1,0:T(4,128)(2,1)S(1)}, u32[]{:S(2)}, u32[]{:S(2)}) %all-to-all-start.2) | async-done | bytes 1048608 | tf_op jit(solution)/shard_map/all_to_all | solution.py:330
  81.3 6.3 %all-to-all-start = ((bf16[64,4,2048]{2,1,0:T(4,128)(2,1)}), bf16[64,4,2048]{2,1,0:T(4,128)(2,1)S(1)}, u32[]{:S(2)}, u32[]{:S(2)}) async-start(bf16[64,4,2048]{2,1,0:T(4,128)(2,1)} %reshape.268), calls=%async_computation | async-start | bytes 2097152 | tf_op jit(solution)/shard_map/all_to_all | solution.py:330
  87.6 1.1 reshape.273
  88.7 1.4 collective-permute-start.22
  90.1 0.9 collective-permute-start.23
  91.0 2.4 slice_bitcast_fusion.2
  93.4 1.5 pad_maximum_fusion
  95.0 1.0 collective-permute-start.14
  95.9 1.5 pad_maximum_fusion.1
  97.5 18.2 %all-to-all-done = bf16[64,4,2048]{2,1,0:T(4,128)(2,1)S(1)} async-done(((bf16[64,4,2048]{2,1,0:T(4,128)(2,1)}), bf16[64,4,2048]{2,1,0:T(4,128)(2,1)S(1)}, u32[]{:S(2)}, u32[]{:S(2)}) %all-to-all-start) | async-done | bytes 1048608 | tf_op jit(solution)/shard_map/all_to_all | solution.py:330
  115.7 1.2 reshape.269
  116.9 1.4 collective-permute-start.12
  118.3 1.6 collective-permute-start.13
  119.9 1.3 constant_dynamic-update-slice_fusion.5
  121.2 1.3 constant_dynamic-update-slice_fusion.4.rows
  122.9 35.4 %collective-permute-done.12 = bf16[256,2048]{1,0:T(8,128)(2,1)S(1)} collective-permute-done((bf16[256,2048]{1,0:T(8,128)(2,1)}, bf16[256,2048]{1,0:T(8,128)(2,1)S(1)}, u32[]{:S(2)}, u32[]{:S(2)}) %collective-permute-start.12) | collective-permute-done | bytes 1048608 | tf_op jit(solution)/shard_map/ppermute | solution.py:30
  158.3 3.0 collective-permute-start.16
  161.5 11.6 %collective-permute-done.16.down_low = bf16[256,2048]{1,0:T(8,128)(2,1)S(1)} collective-permute-done((bf16[256,2048]{1,0:T(8,128)(2,1)S(1)}, bf16[256,2048]{1,0:T(8,128)(2,1)S(1)}, u32[]{:S(2)}, u32[]{:S(2)}) %collective-permute-start.16) | collective-permute-done | bytes 1048608 | tf_op jit(solution)/shard_map/ppermute | solution.py:30
  173.1 2.0 collective-permute-start.18
  175.1 8.7 %shard_map.124 = bf16[512,2048]{1,0:T(8,128)(2,1)S(1)} custom-call(bf16[512,2048]{1,0:T(8,128)(2,1)S(1)} %collective-permute-done.24.rows, bf16[2048,512]{1,0:T(8,128)(2,1)S(1)} %collective-permute-done.14.gu_low, bf16[2048,512]{1,0:T(8,128)(2,1)} %collective-permute-done.15.gu_high, bf16[256,2048]{1,0:T(8,128)(2,1)S(1)} %collective-permute-done.16.down_low, ...), custom_call_target="tpu_custom_call" | custom-call | flops 3221225472 | bytes 10485760 | tf_op jit(solution)/shard_map/pallas_call | solution.py:112
  183.8 3.0 collective-permute-start.25
  186.8 9.0 %shard_map.120 = bf16[512,2048]{1,0:T(8,128)(2,1)} custom-call(bf16[512,2048]{1,0:T(8,128)(2,1)S(1)} %collective-permute-done.18.rows, bf16[2048,512]{1,0:T(8,128)(2,1)S(1)} %collective-permute-done.14.gu_low, bf16[2048,512]{1,0:T(8,128)(2,1)} %collective-permute-done.15.gu_high, bf16[256,2048]{1,0:T(8,128)(2,1)S(1)} %collective-permute-done.16.down_low, ...), custom_call_target="tpu_custom_call" | custom-call | flops 3221225472 | bytes 10485760 | tf_op jit(solution)/shard_map/pallas_call | solution.py:112
  195.8 1.6 copy-done.7
  197.4 7.6 %shard_map.123.a = bf16[512,2048]{1,0:T(8,128)(2,1)S(1)} custom-call(bf16[512,2048]{1,0:T(8,128)(2,1)S(1)} %constant_dynamic-update-slice_fusion.4.rows, bf16[2048,512]{1,0:T(8,128)(2,1)S(1)} %copy-done.7, bf16[2048,512]{1,0:T(8,128)(2,1)} %collective-permute-done.15.gu_high, bf16[256,2048]{1,0:T(8,128)(2,1)S(1)} %collective-permute-done.16.down_low, ...), custom_call_target="tpu_custom_call" | custom-call | flops 3221225472 | bytes 10485760 | tf_op jit(solution)/shard_map/pallas_call | solution.py:112
  206.3 25.5 %collective-permute-done.26.a = bf16[256,2048]{1,0:T(8,128)(2,1)S(1)} collective-permute-done((bf16[256,2048]{1,0:T(8,128)(2,1)S(1)}, bf16[256,2048]{1,0:T(8,128)(2,1)S(1)}, u32[]{:S(2)}, u32[]{:S(2)}) %collective-permute-start.26) | collective-permute-done | bytes 1048608 | tf_op jit(solution)/shard_map/ppermute | solution.py:30
  232.1 1.2 reshape.274
  233.3 10.4 %all-to-all-start.3 = ((bf16[64,4,2048]{2,1,0:T(4,128)(2,1)}), bf16[64,4,2048]{2,1,0:T(4,128)(2,1)}, u32[]{:S(2)}, u32[]{:S(2)}) async-start(bf16[64,4,2048]{2,1,0:T(4,128)(2,1)} %reshape.274), calls=%async_computation.3 | async-start | bytes 2097152 | tf_op jit(solution)/shard_map/all_to_all | solution.py:345
  243.7 1.6 copy-done.5
  245.3 1.6 copy-done.8
  246.9 1.2 copy-done.12
  248.1 7.6 %shard_map.119.a = bf16[512,2048]{1,0:T(8,128)(2,1)S(1)} custom-call(bf16[512,2048]{1,0:T(8,128)(2,1)S(1)} %copy-done.5, bf16[2048,512]{1,0:T(8,128)(2,1)S(1)} %copy-done.8, bf16[2048,512]{1,0:T(8,128)(2,1)} %collective-permute-done.15.gu_high, bf16[256,2048]{1,0:T(8,128)(2,1)S(1)} %copy-done.10, bf16[256,2048]{1,0:T(8,128)(2,1)S(1)} %copy-done.12), custom_call_target="tpu_custom_call" | custom-call | flops 3221225472 | bytes 10485760 | tf_op jit(solution)/shard_map/pallas_call | solution.py:112
  256.3 1.2 collective-permute-start.20
  257.5 24.6 %collective-permute-done.20.a = bf16[256,2048]{1,0:T(8,128)(2,1)S(1)} collective-permute-done((bf16[256,2048]{1,0:T(8,128)(2,1)S(1)}, bf16[256,2048]{1,0:T(8,128)(2,1)S(1)}, u32[]{:S(2)}, u32[]{:S(2)}) %collective-permute-start.20) | collective-permute-done | bytes 1048608 | tf_op jit(solution)/shard_map/ppermute | solution.py:30
  282.4 1.2 reshape.270
  283.6 11.3 %all-to-all-start.1 = ((bf16[64,4,2048]{2,1,0:T(4,128)(2,1)}), bf16[64,4,2048]{2,1,0:T(4,128)(2,1)}, u32[]{:S(2)}, u32[]{:S(2)}) async-start(bf16[64,4,2048]{2,1,0:T(4,128)(2,1)} %reshape.270), calls=%async_computation.1 | async-start | bytes 2097152 | tf_op jit(solution)/shard_map/all_to_all | solution.py:345
  295.2 1.3 reshape.275.second
  296.6 26.4 %all-to-all-done.1 = bf16[64,4,2048]{2,1,0:T(4,128)(2,1)} async-done(((bf16[64,4,2048]{2,1,0:T(4,128)(2,1)}), bf16[64,4,2048]{2,1,0:T(4,128)(2,1)}, u32[]{:S(2)}, u32[]{:S(2)}) %all-to-all-start.1) | async-done | bytes 1048608 | tf_op jit(solution)/shard_map/all_to_all | solution.py:345
  323.0 1.4 reshape.271.first
  324.5 1.1 copy-done.3
  325.6 3.3 %shard_map.127 = bf16[192,2048]{1,0:T(8,128)(2,1)} custom-call(bf16[192,2048]{1,0:T(8,128)(2,1)S(1)} %copy-done.3, bf16[256,2048]{1,0:T(8,128)(2,1)S(1)} %reshape.271.first, bf16[256,2048]{1,0:T(8,128)(2,1)S(1)} %reshape.275.second, s32[192,4]{1,0:T(8,128)S(1)} %copy.29.places, f32[192,2]{1,0:T(8,128)S(1)} %copy.30.weight), custom_call_target="tpu_custom_call" | custom-call | flops 805306368 | bytes 3670016 | tf_op jit(solution)/shard_map/pallas_call | solution.py:174
  (101 shorter events, 7.6 us)
Async XLA Ops:
  0.0 1.2 copy-start
  0.0 13.0 %copy-start.16 = (bf16[768,256]{1,0:T(8,128)(2,1)S(1)}, bf16[768,256]{1,0:T(8,128)(2,1)}, u32[]{:S(2)}) copy-start(bf16[768,256]{1,0:T(8,128)(2,1)} %param.12) | copy-start | bytes 1179652
  0.0 13.0 %copy-start.15 = (bf16[768,256]{1,0:T(8,128)(2,1)S(1)}, bf16[768,256]{1,0:T(8,128)(2,1)}, u32[]{:S(2)}) copy-start(bf16[768,256]{1,0:T(8,128)(2,1)} %param.13) | copy-start | bytes 1179652
  0.0 13.1 %copy-start.20 = (f32[3,256]{1,0:T(4,128)S(1)}, f32[3,256]{1,0:T(4,128)}, u32[]{:S(2)}) copy-start(f32[3,256]{1,0:T(4,128)} %param.15) | copy-start | bytes 9220
  0.0 13.1 %copy-start.19 = (s32[192,2]{0,1:T(2,128)S(1)}, s32[192,2]{0,1:T(2,128)}, u32[]{:S(2)}) copy-start(s32[192,2]{0,1:T(2,128)} %param.19) | copy-start | bytes 4612
  0.0 14.8 %copy-start.18 = (bf16[768,256]{1,0:T(8,128)(2,1)S(1)}, bf16[768,256]{1,0:T(8,128)(2,1)}, u32[]{:S(2)}) copy-start(bf16[768,256]{1,0:T(8,128)(2,1)} %param.14) | copy-start | bytes 1179652
  1.3 19.2 %collective-permute-start.6 = (bf16[128,2048]{1,0:T(8,128)(2,1)S(1)}, bf16[128,2048]{1,0:T(8,128)(2,1)}, u32[]{:S(2)}, u32[]{:S(2)}) collective-permute-start(bf16[128,2048]{1,0:T(8,128)(2,1)S(1)} %constant_dynamic-slice_fusion), channel_id=1, source_target_pairs={{0,1},{1,2},{2,3},{3,0},{4,5},{5,6},{6,7},{7,4},{8,9},{9,10},{10,1... | collective-permute-start | bytes 1572872 | tf_op jit(solution)/shard_map/ppermute | solution.py:17
  3.5 15.8 %collective-permute-start.3 = (bf16[128,2048]{1,0:T(8,128)(2,1)S(1)}, bf16[128,2048]{1,0:T(8,128)(2,1)}, u32[]{:S(2)}, u32[]{:S(2)}) collective-permute-start(bf16[128,2048]{1,0:T(8,128)(2,1)S(1)} %constant_dynamic-slice_fusion), channel_id=1, source_target_pairs={{0,3},{1,0},{2,1},{3,2},{4,7},{5,4},{6,5},{7,6},{8,11},{9,8},{10,9... | collective-permute-start | bytes 1572872 | tf_op jit(solution)/shard_map/ppermute | solution.py:17
  6.3 7.2 %collective-permute-start.1 = (bf16[2,1,256]{2,1,0:T(2,128)(2,1)}, bf16[2,1,256]{2,1,0:T(2,128)(2,1)}, u32[]{:S(2)}, u32[]{:S(2)}) collective-permute-start(bf16[2,1,256]{2,1,0:T(2,128)(2,1)} %get-tuple-element.26), channel_id=1, source_target_pairs={{4,0},{8,4},{12,8},{16,12},{20,16},{24,20},{28,24},{32,28},{36,32}... | collective-permute-start | bytes 3080 | tf_op jit(solution)/shard_map/ppermute | solution.py:283
  11.0 3.2 collective-permute-start
  15.3 7.5 %collective-permute-start.5 = (bf16[192,256]{1,0:T(8,128)(2,1)S(1)}, bf16[192,256]{1,0:T(8,128)(2,1)S(1)}, u32[]{:S(2)}, u32[]{:S(2)}) collective-permute-start(bf16[192,256]{1,0:T(8,128)(2,1)S(1)} %get-tuple-element.29), channel_id=1, source_target_pairs={{0,1},{1,2},{2,3},{3,0},{4,5},{5,6},{6,7},{7,4},{8,9},{9,10},{10,1... | collective-permute-start | bytes 294920 | tf_op jit(solution)/shard_map/ppermute | solution.py:17
  15.4 18.0 %collective-permute-start.8 = (bf16[192,256]{1,0:T(8,128)(2,1)S(1)}, bf16[192,256]{1,0:T(8,128)(2,1)S(1)}, u32[]{:S(2)}, u32[]{:S(2)}) collective-permute-start(bf16[192,256]{1,0:T(8,128)(2,1)S(1)} %get-tuple-element.30), channel_id=1, source_target_pairs={{0,2},{1,3},{2,0},{3,1},{4,6},{5,7},{6,4},{7,5},{8,10},{9,11},{10,... | collective-permute-start | bytes 294920 | tf_op jit(solution)/shard_map/ppermute | solution.py:17
  17.4 14.2 %collective-permute-start.2 = (bf16[192,256]{1,0:T(8,128)(2,1)S(1)}, bf16[192,256]{1,0:T(8,128)(2,1)S(1)}, u32[]{:S(2)}, u32[]{:S(2)}) collective-permute-start(bf16[192,256]{1,0:T(8,128)(2,1)S(1)} %get-tuple-element.27), channel_id=1, source_target_pairs={{0,3},{1,0},{2,1},{3,2},{4,7},{5,4},{6,5},{7,6},{8,11},{9,8},{10,9... | collective-permute-start | bytes 294920 | tf_op jit(solution)/shard_map/ppermute | solution.py:17
  20.2 8.4 %collective-permute-start.9 = (bf16[64,2048]{1,0:T(8,128)(2,1)S(1)}, bf16[64,2048]{1,0:T(8,128)(2,1)S(1)}, u32[]{:S(2)}, u32[]{:S(2)}) collective-permute-start(bf16[64,2048]{1,0:T(8,128)(2,1)S(1)} %slice.141), channel_id=1, source_target_pairs={{0,3},{1,0},{2,1},{3,2},{4,7},{5,4},{6,5},{7,6},{8,11},{9,8},{10,9... | collective-permute-start | bytes 786440 | tf_op jit(solution)/shard_map/ppermute | solution.py:17
  21.5 8.6 %collective-permute-start.10 = (bf16[64,2048]{1,0:T(8,128)(2,1)S(1)}, bf16[64,2048]{1,0:T(8,128)(2,1)S(1)}, u32[]{:S(2)}, u32[]{:S(2)}) collective-permute-start(bf16[64,2048]{1,0:T(8,128)(2,1)S(1)} %slice.142), channel_id=1, source_target_pairs={{0,1},{1,2},{2,3},{3,0},{4,5},{5,6},{6,7},{7,4},{8,9},{9,10},{10,1... | collective-permute-start | bytes 786440 | tf_op jit(solution)/shard_map/ppermute | solution.py:17
  22.8 10.2 %collective-permute-start.7 = (bf16[128,2048]{1,0:T(8,128)(2,1)}, bf16[128,2048]{1,0:T(8,128)(2,1)S(1)}, u32[]{:S(2)}, u32[]{:S(2)}) collective-permute-start(bf16[128,2048]{1,0:T(8,128)(2,1)} %collective-permute-done.6), channel_id=1, source_target_pairs={{0,4},{4,0},{8,12},{12,8},{16,20},{20,16},{24,28},{28,24},{32,36},... | collective-permute-start | bytes 1572872 | tf_op jit(solution)/shard_map/ppermute | solution.py:21
  28.6 5.5 %collective-permute-start.4 = (bf16[128,2048]{1,0:T(8,128)(2,1)}, bf16[128,2048]{1,0:T(8,128)(2,1)S(1)}, u32[]{:S(2)}, u32[]{:S(2)}) collective-permute-start(bf16[128,2048]{1,0:T(8,128)(2,1)} %collective-permute-done.3), channel_id=1, source_target_pairs={{0,4},{4,0},{8,12},{12,8},{16,20},{20,16},{24,28},{28,24},{32,36},... | collective-permute-start | bytes 1572872 | tf_op jit(solution)/shard_map/ppermute | solution.py:21
  30.2 3.2 collective-permute-start.11
  33.8 1.1 copy-start.17
  34.1 1.4 copy-start.13
  38.3 0.9 copy-start.2
  40.4 40.9 %all-to-all-start.2 = ((bf16[64,4,2048]{2,1,0:T(4,128)(2,1)}), bf16[64,4,2048]{2,1,0:T(4,128)(2,1)S(1)}, u32[]{:S(2)}, u32[]{:S(2)}) async-start(bf16[64,4,2048]{2,1,0:T(4,128)(2,1)} %reshape.272), calls=%async_computation.2 | async-start | bytes 2097152 | tf_op jit(solution)/shard_map/all_to_all | solution.py:330
  81.3 34.4 %all-to-all-start = ((bf16[64,4,2048]{2,1,0:T(4,128)(2,1)}), bf16[64,4,2048]{2,1,0:T(4,128)(2,1)S(1)}, u32[]{:S(2)}, u32[]{:S(2)}) async-start(bf16[64,4,2048]{2,1,0:T(4,128)(2,1)} %reshape.268), calls=%async_computation | async-start | bytes 2097152 | tf_op jit(solution)/shard_map/all_to_all | solution.py:330
  88.7 29.6 %collective-permute-start.22 = (bf16[256,2048]{1,0:T(8,128)(2,1)}, bf16[256,2048]{1,0:T(8,128)(2,1)}, u32[]{:S(2)}, u32[]{:S(2)}) collective-permute-start(bf16[256,2048]{1,0:T(8,128)(2,1)} %reshape.273), channel_id=1, source_target_pairs={{4,7},{1,0},{6,5},{3,2},{0,6},{5,3},{2,4},{7,1},{12,15},{9,8},{14,... | collective-permute-start | bytes 3145736 | tf_op jit(solution)/shard_map/ppermute | solution.py:30
  90.1 31.2 %collective-permute-start.23 = (bf16[256,2048]{1,0:T(8,128)(2,1)}, bf16[256,2048]{1,0:T(8,128)(2,1)}, u32[]{:S(2)}, u32[]{:S(2)}) collective-permute-start(bf16[256,2048]{1,0:T(8,128)(2,1)} %reshape.273), channel_id=1, source_target_pairs={{4,5},{1,2},{6,7},{3,0},{0,4},{5,1},{2,6},{7,3},{12,13},{9,10},{14... | collective-permute-start | bytes 3145736 | tf_op jit(solution)/shard_map/ppermute | solution.py:30
  95.0 80.1 %collective-permute-start.14 = (bf16[2048,512]{1,0:T(8,128)(2,1)}, bf16[2048,512]{1,0:T(8,128)(2,1)S(1)}, u32[]{:S(2)}, u32[]{:S(2)}) collective-permute-start(bf16[2048,512]{1,0:T(8,128)(2,1)} %pad_maximum_fusion), channel_id=1, source_target_pairs={{0,4},{5,1},{2,6},{7,3},{4,7},{1,0},{6,5},{3,2},{8,12},{13,9},{10,... | collective-permute-start | bytes 6291464 | tf_op jit(solution)/shard_map/ppermute | solution.py:30
  97.5 77.6 %collective-permute-start.15 = (bf16[2048,512]{1,0:T(8,128)(2,1)}, bf16[2048,512]{1,0:T(8,128)(2,1)}, u32[]{:S(2)}, u32[]{:S(2)}) collective-permute-start(bf16[2048,512]{1,0:T(8,128)(2,1)} %pad_maximum_fusion.1), channel_id=1, source_target_pairs={{0,4},{5,1},{2,6},{7,3},{4,5},{1,2},{6,7},{3,0},{8,12},{13,9},{10,... | collective-permute-start | bytes 6291464 | tf_op jit(solution)/shard_map/ppermute | solution.py:30
  116.9 5.7 %copy-start.14 = (bf16[1,512,2048]{2,1,0:T(8,128)(2,1)S(1)}, bf16[1,512,2048]{2,1,0:T(8,128)(2,1)}, u32[]{:S(2)}) copy-start(bf16[1,512,2048]{2,1,0:T(8,128)(2,1)} %param.23) | copy-start | bytes 6291460
  116.9 41.4 %collective-permute-start.12 = (bf16[256,2048]{1,0:T(8,128)(2,1)}, bf16[256,2048]{1,0:T(8,128)(2,1)S(1)}, u32[]{:S(2)}, u32[]{:S(2)}) collective-permute-start(bf16[256,2048]{1,0:T(8,128)(2,1)} %reshape.269), channel_id=1, source_target_pairs={{4,7},{1,0},{6,5},{3,2},{0,6},{5,3},{2,4},{7,1},{12,15},{9,8},{14,... | collective-permute-start | bytes 3145736 | tf_op jit(solution)/shard_map/ppermute | solution.py:30
  118.3 43.0 %collective-permute-start.13 = (bf16[256,2048]{1,0:T(8,128)(2,1)}, bf16[256,2048]{1,0:T(8,128)(2,1)S(1)}, u32[]{:S(2)}, u32[]{:S(2)}) collective-permute-start(bf16[256,2048]{1,0:T(8,128)(2,1)} %reshape.269), channel_id=1, source_target_pairs={{4,5},{1,2},{6,7},{3,0},{0,4},{5,1},{2,6},{7,3},{12,13},{9,10},{14... | collective-permute-start | bytes 3145736 | tf_op jit(solution)/shard_map/ppermute | solution.py:30
  122.6 52.5 %collective-permute-start.24 = (bf16[512,2048]{1,0:T(8,128)(2,1)S(1)}, bf16[512,2048]{1,0:T(8,128)(2,1)S(1)}, u32[]{:S(2)}, u32[]{:S(2)}) collective-permute-start(bf16[512,2048]{1,0:T(8,128)(2,1)S(1)} %constant_dynamic-update-slice_fusion.4.rows), channel_id=1, source_target_pairs={{0,4},{4,0},{8,12},{12,8},{16,20},{20,16},{24,28},{28,24},{32,36},... | collective-permute-start | bytes 6291464 | tf_op jit(solution)/shard_map/ppermute | solution.py:21
  158.3 14.8 %collective-permute-start.16 = (bf16[256,2048]{1,0:T(8,128)(2,1)S(1)}, bf16[256,2048]{1,0:T(8,128)(2,1)S(1)}, u32[]{:S(2)}, u32[]{:S(2)}) collective-permute-start(bf16[256,2048]{1,0:T(8,128)(2,1)S(1)} %get-tuple-element.20), channel_id=1, source_target_pairs={{0,4},{5,1},{2,6},{7,3},{4,7},{1,0},{6,5},{3,2},{8,12},{13,9},{10,... | collective-permute-start | bytes 3145736 | tf_op jit(solution)/shard_map/ppermute | solution.py:30
  161.3 13.7 %collective-permute-start.17 = (bf16[256,2048]{1,0:T(8,128)(2,1)S(1)}, bf16[256,2048]{1,0:T(8,128)(2,1)S(1)}, u32[]{:S(2)}, u32[]{:S(2)}) collective-permute-start(bf16[256,2048]{1,0:T(8,128)(2,1)S(1)} %get-tuple-element.19), channel_id=1, source_target_pairs={{0,4},{5,1},{2,6},{7,3},{4,5},{1,2},{6,7},{3,0},{8,12},{13,9},{10,... | collective-permute-start | bytes 3145736 | tf_op jit(solution)/shard_map/ppermute | solution.py:30
  161.5 22.4 %copy-start.4 = (bf16[512,2048]{1,0:T(8,128)(2,1)}, bf16[512,2048]{1,0:T(8,128)(2,1)S(1)}, u32[]{:S(2)}) copy-start(bf16[512,2048]{1,0:T(8,128)(2,1)S(1)} %constant_dynamic-update-slice_fusion.2.rows) | copy-start | bytes 6291460
  173.1 22.8 %copy-start.9 = (bf16[256,2048]{1,0:T(8,128)(2,1)}, bf16[256,2048]{1,0:T(8,128)(2,1)S(1)}, u32[]{:S(2)}) copy-start(bf16[256,2048]{1,0:T(8,128)(2,1)S(1)} %collective-permute-done.16.down_low) | copy-start | bytes 3145732
  173.1 13.7 %collective-permute-start.18 = (bf16[512,2048]{1,0:T(8,128)(2,1)S(1)}, bf16[512,2048]{1,0:T(8,128)(2,1)S(1)}, u32[]{:S(2)}, u32[]{:S(2)}) collective-permute-start(bf16[512,2048]{1,0:T(8,128)(2,1)S(1)} %constant_dynamic-update-slice_fusion.2.rows), channel_id=1, source_target_pairs={{0,4},{4,0},{8,12},{12,8},{16,20},{20,16},{24,28},{28,24},{32,36},... | collective-permute-start | bytes 6291464 | tf_op jit(solution)/shard_map/ppermute | solution.py:21
  175.0 20.8 %copy-start.11 = (bf16[256,2048]{1,0:T(8,128)(2,1)}, bf16[256,2048]{1,0:T(8,128)(2,1)S(1)}, u32[]{:S(2)}) copy-start(bf16[256,2048]{1,0:T(8,128)(2,1)S(1)} %collective-permute-done.17.down_high) | copy-start | bytes 3145732
  175.1 11.7 %copy-start.6 = (bf16[2048,512]{1,0:T(8,128)(2,1)}, bf16[2048,512]{1,0:T(8,128)(2,1)S(1)}, u32[]{:S(2)}) copy-start(bf16[2048,512]{1,0:T(8,128)(2,1)S(1)} %collective-permute-done.14.gu_low) | copy-start | bytes 6291460
  183.8 21.2 %collective-permute-start.25 = (bf16[512,2048]{1,0:T(8,128)(2,1)S(1)}, bf16[512,2048]{1,0:T(8,128)(2,1)S(1)}, u32[]{:S(2)}, u32[]{:S(2)}) collective-permute-start(bf16[512,2048]{1,0:T(8,128)(2,1)S(1)} %shard_map.124), channel_id=1, source_target_pairs={{0,4},{4,0},{8,12},{12,8},{16,20},{20,16},{24,28},{28,24},{32,36},... | collective-permute-start | bytes 6291464 | tf_op jit(solution)/shard_map/ppermute | solution.py:21
  195.8 60.0 %collective-permute-start.19 = (bf16[512,2048]{1,0:T(8,128)(2,1)}, bf16[512,2048]{1,0:T(8,128)(2,1)S(1)}, u32[]{:S(2)}, u32[]{:S(2)}) collective-permute-start(bf16[512,2048]{1,0:T(8,128)(2,1)} %shard_map.120), channel_id=1, source_target_pairs={{0,4},{4,0},{8,12},{12,8},{16,20},{20,16},{24,28},{28,24},{32,36},... | collective-permute-start | bytes 6291464 | tf_op jit(solution)/shard_map/ppermute | solution.py:21
  195.8 1.6 copy-start.7
  205.6 26.2 %collective-permute-start.26 = (bf16[256,2048]{1,0:T(8,128)(2,1)S(1)}, bf16[256,2048]{1,0:T(8,128)(2,1)S(1)}, u32[]{:S(2)}, u32[]{:S(2)}) collective-permute-start(bf16[256,2048]{1,0:T(8,128)(2,1)S(1)} %get-tuple-element.15), channel_id=1, source_target_pairs={{7,4},{0,1},{5,6},{2,3},{6,0},{3,5},{4,2},{1,7},{15,12},{8,9},{13,... | collective-permute-start | bytes 3145736 | tf_op jit(solution)/shard_map/ppermute | solution.py:30
  206.0 25.8 %collective-permute-start.27 = (bf16[256,2048]{1,0:T(8,128)(2,1)S(1)}, bf16[256,2048]{1,0:T(8,128)(2,1)S(1)}, u32[]{:S(2)}, u32[]{:S(2)}) collective-permute-start(bf16[256,2048]{1,0:T(8,128)(2,1)S(1)} %get-tuple-element.16), channel_id=1, source_target_pairs={{5,4},{2,1},{7,6},{0,3},{4,0},{1,5},{6,2},{3,7},{13,12},{10,9},{15... | collective-permute-start | bytes 3145736 | tf_op jit(solution)/shard_map/ppermute | solution.py:30
  233.3 10.4 %copy-start.10 = (bf16[256,2048]{1,0:T(8,128)(2,1)S(1)}, bf16[256,2048]{1,0:T(8,128)(2,1)}, u32[]{:S(2)}) copy-start(bf16[256,2048]{1,0:T(8,128)(2,1)} %copy-done.9) | copy-start | bytes 3145732
  233.3 50.3 %all-to-all-start.3 = ((bf16[64,4,2048]{2,1,0:T(4,128)(2,1)}), bf16[64,4,2048]{2,1,0:T(4,128)(2,1)}, u32[]{:S(2)}, u32[]{:S(2)}) async-start(bf16[64,4,2048]{2,1,0:T(4,128)(2,1)} %reshape.274), calls=%async_computation.3 | async-start | bytes 2097152 | tf_op jit(solution)/shard_map/all_to_all | solution.py:345
  243.7 1.6 copy-start.5
  245.3 1.6 copy-start.8
  246.9 1.2 copy-start.12
  256.3 25.8 %collective-permute-start.20 = (bf16[256,2048]{1,0:T(8,128)(2,1)S(1)}, bf16[256,2048]{1,0:T(8,128)(2,1)S(1)}, u32[]{:S(2)}, u32[]{:S(2)}) collective-permute-start(bf16[256,2048]{1,0:T(8,128)(2,1)S(1)} %get-tuple-element.12), channel_id=1, source_target_pairs={{7,4},{0,1},{5,6},{2,3},{6,0},{3,5},{4,2},{1,7},{15,12},{8,9},{13,... | collective-permute-start | bytes 3145736 | tf_op jit(solution)/shard_map/ppermute | solution.py:30
  257.5 24.6 %collective-permute-start.21 = (bf16[256,2048]{1,0:T(8,128)(2,1)S(1)}, bf16[256,2048]{1,0:T(8,128)(2,1)S(1)}, u32[]{:S(2)}, u32[]{:S(2)}) collective-permute-start(bf16[256,2048]{1,0:T(8,128)(2,1)S(1)} %get-tuple-element.13), channel_id=1, source_target_pairs={{5,4},{2,1},{7,6},{0,3},{4,0},{1,5},{6,2},{3,7},{13,12},{10,9},{15... | collective-permute-start | bytes 3145736 | tf_op jit(solution)/shard_map/ppermute | solution.py:30
  282.4 12.7 %copy-start.21 = (f32[192,2]{0,1:T(2,128)S(1)}, f32[192,2]{0,1:T(2,128)}, u32[]{:S(2)}) copy-start(f32[192,2]{0,1:T(2,128)} %param.20) | copy-start | bytes 4612
  283.6 39.4 %all-to-all-start.1 = ((bf16[64,4,2048]{2,1,0:T(4,128)(2,1)}), bf16[64,4,2048]{2,1,0:T(4,128)(2,1)}, u32[]{:S(2)}, u32[]{:S(2)}) async-start(bf16[64,4,2048]{2,1,0:T(4,128)(2,1)} %reshape.270), calls=%async_computation.1 | async-start | bytes 2097152 | tf_op jit(solution)/shard_map/all_to_all | solution.py:345
  323.0 5.9 %copy-start.1 = (bf16[256,2048]{1,0:T(8,128)(2,1)S(1)}, bf16[256,2048]{1,0:T(8,128)(2,1)}, u32[]{:S(2)}) copy-start(bf16[256,2048]{1,0:T(8,128)(2,1)} %param.16) | copy-start | bytes 3145732
  324.4 1.1 copy-start.3
